TPU v7x, 512 devices: a whole 4x4x16 slice. The times are simulated.
512 devices in a mesh: sp: 16 (over z), dp: 32 (over y, x, core).
Axes of the slice: x: 4, y: 4, z: 16, core: 2. Of those that a mesh axis runs over, the one named last changes fastest.
Arguments:
- cotangent: bfloat16 [32, 2048, 2048], P('dp', 'sp'), may hold values from -6 to 6
- unit_pre: bfloat16 [32, 2048, 2048], P('dp', None, 'sp'), may hold values from -6 to 6
- gate_pre: bfloat16 [32, 2048, 2048], P('dp', None, 'sp'), may hold values from -15 to 15
- out_weight: bfloat16 [2048, 2048], P('dp', 'sp'), may hold values from -0.125 to 0.125
- mix_weight: bfloat16 [8, 128, 128], replicated, may hold values from -0.5 to 0.5
- mix_bias: bfloat16 [8, 128], replicated, may hold values from 0.099609375 to 1.8984375
- norm_gain: bfloat16 [2048], P('sp'), may hold values from 0.099609375 to 1.8984375
- norm_shift: bfloat16 [2048], P('sp'), may hold values from -3 to 3
Outputs:
- unit_grad: bfloat16 [32, 2048, 2048], P('dp', None, 'sp')
- gate_grad: bfloat16 [32, 2048, 2048], P('dp', None, 'sp')
- out_weight_grad: float32 [2048, 2048], P('dp', 'sp')
- mix_weight_grad: float32 [8, 128, 128], replicated
- mix_bias_grad: float32 [8, 128], replicated
- gain_grad: float32 [2048], P('sp')
- shift_grad: float32 [2048], P('sp')
All inputs are finite; a program needn't handle non-finite values.
Results may differ from a plain program's by a relative error of at most 0.015.
Values may be sent and summed in bfloat16 or wider, within the bound.
A program may use at most 64 MiB of HBM per device.

v0:
```python
import math
import jax
import jax.numpy as jnp
from jax import lax
from jax.sharding import PartitionSpec as P

GW = 2048
GROUPS = 8
BLK = 128
epsilon = 1e-05
tanh_coef = math.sqrt(2.0 / math.pi)


def sum_over(x, axis):
    devices = lax.axis_size(axis)
    copies = jnp.broadcast_to(x[None], (devices, *x.shape))
    return lax.all_to_all(copies, axis, 0, 0, tiled=True).sum(axis=0)


def gelu_slope(values):
    inner = tanh_coef * (values + 0.044715 * values * values * values)
    hyper = jnp.tanh(inner)
    return 0.5 * (1.0 + hyper) + 0.5 * values * (1.0 - hyper * hyper) * tanh_coef * (
        1.0 + 3.0 * 0.044715 * values * values
    )


def local(cotangent, unit_pre, gate_pre, out_weight, mix_weight, mix_bias, norm_gain, norm_shift):
    seq_len = unit_pre.shape[1]
    channels = unit_pre.shape[2]
    group_dim = GW // GROUPS
    blocks = seq_len // BLK
    sp_size = lax.axis_size("sp")
    sp_at = lax.axis_index("sp")
    group = sp_at * channels // group_dim
    weight_rows = lax.all_gather(out_weight, "sp", axis=1, tiled=True)
    weight_whole = lax.all_gather(weight_rows, "dp", axis=0, tiled=True)
    units = unit_pre[0].astype(jnp.float32)
    gates = gate_pre[0].astype(jnp.float32)
    unit_act = jax.nn.gelu(units)
    gate_act = jax.nn.gelu(gates)
    moments = sum_over(
        jnp.stack([jnp.sum(gate_act, axis=-1), jnp.sum(gate_act * gate_act, axis=-1)]), "sp"
    )
    mean_val = moments[0] / GW
    var_val = moments[1] / GW - mean_val * mean_val
    rstd_val = lax.rsqrt(var_val + epsilon)
    centred = (gate_act - mean_val[:, None]) * rstd_val[:, None]
    gain_vec = norm_gain.astype(jnp.float32)
    normed = (centred * gain_vec + norm_shift.astype(jnp.float32)).astype(jnp.bfloat16)
    causal = jnp.arange(BLK)[:, None] >= jnp.arange(BLK)[None, :]
    local_weight = lax.dynamic_index_in_dim(mix_weight, group, 0, keepdims=False)
    masked = jnp.where(causal, local_weight, jnp.zeros_like(local_weight))
    local_bias = lax.dynamic_index_in_dim(mix_bias, group, 0, keepdims=False).astype(jnp.float32)
    normed_blocks = normed.reshape(blocks, BLK, channels)
    mixed = jnp.einsum("ts,nsd->ntd", masked, normed_blocks, preferred_element_type=jnp.float32)
    mixed = (mixed + local_bias[None, :, None]).reshape(seq_len, channels)
    gated = (unit_act * mixed).astype(jnp.bfloat16)
    gated_rows = lax.all_to_all(gated, "sp", split_axis=0, concat_axis=1, tiled=True)
    head_rows = jnp.dot(cotangent[0], weight_whole, preferred_element_type=jnp.float32)
    head = lax.all_to_all(
        head_rows.astype(jnp.bfloat16), "sp", split_axis=1, concat_axis=0, tiled=True
    ).astype(jnp.float32)
    weight_part = lax.dot_general(
        cotangent[0], gated_rows, (((0,), (0,)), ((), ())), preferred_element_type=jnp.float32
    ).astype(jnp.bfloat16)
    token_count = lax.axis_size("dp") * seq_len
    norm_scale = 1.0 / math.sqrt(token_count)
    mix_scale = 1.0 / math.sqrt(token_count // BLK * group_dim)
    plane_sum = lax.psum_scatter(weight_part, "dp", scatter_dimension=0, tiled=True)
    plane_parts = jnp.moveaxis(plane_sum.reshape(plane_sum.shape[0], sp_size, channels), 1, 0)
    arrived = lax.all_to_all(plane_parts, "sp", split_axis=0, concat_axis=0, tiled=True)
    out_grad = arrived.astype(jnp.float32).sum(axis=0) * norm_scale
    unit_grad = (head * mixed * gelu_slope(units)).astype(jnp.bfloat16)
    mix_grad = head * unit_act
    mix_round = mix_grad.astype(jnp.bfloat16).reshape(blocks, BLK, channels)
    mix_term = jnp.einsum(
        "ntd,nsd->ts", mix_round, normed_blocks, preferred_element_type=jnp.float32
    )
    mix_term = jnp.where(causal, mix_term, jnp.float32(0.0))
    bias_term = jnp.sum(mix_grad.reshape(blocks, BLK, channels), axis=(0, 2))
    normed_grad = jnp.einsum(
        "ts,ntd->nsd", masked, mix_round, preferred_element_type=jnp.float32
    ).reshape(seq_len, channels)
    gain_term = jnp.sum(normed_grad * centred, axis=0)
    shift_term = jnp.sum(normed_grad, axis=0)
    scaled = normed_grad * gain_vec
    back_sums = sum_over(
        jnp.stack([jnp.sum(scaled, axis=-1), jnp.sum(scaled * centred, axis=-1)]), "sp"
    )
    first_m = back_sums[0] / GW
    second_m = back_sums[1] / GW
    gate_grad = (
        rstd_val[:, None]
        * (scaled - first_m[:, None] - centred * second_m[:, None])
        * gelu_slope(gates)
    ).astype(jnp.bfloat16)
    group_hot = (jnp.arange(GROUPS) == group).astype(jnp.float32)
    own_hot = (jnp.arange(sp_size) == sp_at).astype(jnp.float32)
    packed = jnp.concatenate(
        [
            (group_hot[:, None, None] * mix_term).reshape(GROUPS * BLK, BLK),
            group_hot[:, None] * bias_term,
            own_hot[:, None] * gain_term,
            own_hot[:, None] * shift_term,
        ]
    )
    total = lax.psum(packed, ("sp", "dp"))
    top = GROUPS * BLK
    weight_total = total[:top].reshape(GROUPS, BLK, BLK)
    bias_total = total[top : top + GROUPS]
    tail = total[top + GROUPS :]
    gain_total = lax.dynamic_index_in_dim(tail, sp_at, 0, keepdims=False)
    shift_total = lax.dynamic_index_in_dim(tail, sp_size + sp_at, 0, keepdims=False)
    return (
        unit_grad[None],
        gate_grad[None],
        out_grad,
        weight_total * mix_scale,
        bias_total * mix_scale,
        gain_total * norm_scale,
        shift_total * norm_scale,
    )


def solution(mesh):
    return jax.shard_map(
        local,
        mesh=mesh,
        in_specs=(
            P("dp", "sp", None),
            P("dp", None, "sp"),
            P("dp", None, "sp"),
            P("dp", "sp"),
            P(),
            P(),
            P("sp"),
            P("sp"),
        ),
        out_specs=(
            P("dp", None, "sp"),
            P("dp", None, "sp"),
            P("dp", "sp"),
            P(),
            P(),
            P("sp"),
            P("sp"),
        ),
        check_vma=False,
    )
```

profile of v0, /device:TPU:32, one launch (start us, length us, event | category | flops | bytes accessed | tf_op | source)
XLA Modules:
  0.0 828.7 jit_solution(9951408123859522207)
XLA Ops:
  7.2 0.0 all-gather.2.cloned.1.call-start
  7.2 37.3 %all_gather.6 = bf16[64,2048]{1,0:T(8,128)(2,1)} all-gather(bf16[64,128]{1,0:T(8,128)(2,1)} %param.11), channel_id=1, replica_groups=mesh['sp'=16,'dp'=32] {'sp'}, dimensions={1}, use_global_device_ids=true | all-gather | bytes 278528 | tf_op jit(solution)/shard_map/all_gather | solution.py:36
  44.6 0.0 all-gather.2.cloned.1.call-update
  44.6 1.8 fusion.58
  46.4 0.8 broadcast_in_dim.11
  47.2 8.9 %all-to-all-start.1 = ((f32[16,2,2048]{2,1,0:T(2,128)}), f32[16,2,2048]{2,1,0:T(2,128)S(1)}, u32[]{:S(2)}, u32[]{:S(2)}) async-start(f32[16,2,2048]{2,1,0:T(2,128)} %broadcast_in_dim.11), calls=%async_computation.1 | async-start | bytes 524288 | tf_op jit(solution)/shard_map/all_to_all | solution.py:17
  56.1 54.5 %all-gather.2.cloned.1.call-done = bf16[2048,2048]{1,0:T(8,128)(2,1)} async-done(((bf16[64,2048]{1,0:T(8,128)(2,1)}), bf16[2048,2048]{1,0:T(8,128)(2,1)}) %all-gather.2.cloned.1.call-update) | async-done | bytes 8388624 | tf_op jit(solution)/shard_map/all_gather | solution.py:37
  110.6 4.6 fusion.5
  115.3 0.9 copy.53
  116.2 12.7 %all-to-all-start = ((bf16[128,16,128]{2,0,1:T(8,128)(2,1)}), bf16[128,16,128]{2,0,1:T(8,128)(2,1)S(1)}, u32[]{:S(2)}, u32[]{:S(2)}) async-start(bf16[128,16,128]{2,0,1:T(8,128)(2,1)} %bitcast.135), calls=%async_computation | async-start | bytes 1048576 | tf_op jit(solution)/shard_map/all_to_all | solution.py:61
  128.9 0.1 reduce_sum.92
  129.0 29.5 %all-to-all-done = bf16[128,16,128]{2,0,1:T(8,128)(2,1)S(1)} async-done(((bf16[128,16,128]{2,0,1:T(8,128)(2,1)}), bf16[128,16,128]{2,0,1:T(8,128)(2,1)S(1)}, u32[]{:S(2)}, u32[]{:S(2)}) %all-to-all-start) | async-done | bytes 524320 | tf_op jit(solution)/shard_map/all_to_all | solution.py:61
  158.6 0.5 fusion.59
  159.1 1.0 copy-done.3
  160.1 3.3 fusion.56
  163.4 0.8 broadcast_in_dim.15
  164.2 6.1 all-to-all-start.2
  170.3 0.7 fusion.80
  171.0 17.5 %all-to-all-done.2 = f32[16,2,2048]{2,1,0:T(2,128)S(1)} async-done(((f32[16,2,2048]{2,1,0:T(2,128)}), f32[16,2,2048]{2,1,0:T(2,128)S(1)}, u32[]{:S(2)}, u32[]{:S(2)}) %all-to-all-start.2) | async-done | bytes 262176 | tf_op jit(solution)/shard_map/all_to_all | solution.py:17
  188.6 0.1 reduce_sum.95
  188.7 2.8 fusion.51
  191.5 3.0 multiply_convert_fusion
  194.4 6.1 all-to-all-start.3
  200.5 0.0 all-reduce.2.cloned.1.call-start
  200.6 0.3 reduce_sum.99
  200.8 0.1 broadcast_bitcast_fusion
  200.9 2.5 fusion.6
  203.5 0.2 bitcast_multiply_fusion.5
  203.7 0.1 broadcast_multiply_fusion.2
  203.7 0.8 pad_maximum_fusion
  204.6 0.0 reduce-scatter.4.cloned.1.call-start
  204.6 24.2 %all-to-all-done.3 = bf16[16,128,128]{2,1,0:T(8,128)(2,1)S(1)} async-done(((bf16[16,128,128]{2,1,0:T(8,128)(2,1)}), bf16[16,128,128]{2,1,0:T(8,128)(2,1)S(1)}, u32[]{:S(2)}, u32[]{:S(2)}) %all-to-all-start.3) | async-done | bytes 524320 | tf_op jit(solution)/shard_map/all_to_all | solution.py:59
  228.9 0.3 copy.36
  229.2 5.5 convert_bitcast_fusion
  234.7 12.4 %copy.42 = bf16[2048,2048]{1,0:T(8,128)(2,1)} copy(bf16[2048,2048]{0,1:T(8,128)(2,1)} %convert_bitcast_fusion) | data formatting | bytes 16777216
  247.1 423.4 %all-reduce.2.cloned.1.call-done = f32[1064,128]{1,0:T(8,128)} async-done(((f32[1064,128]{1,0:T(8,128)}), f32[1064,128]{1,0:T(8,128)}) %all-reduce.2.cloned.1.call-update) | async-done | bytes 544784 | tf_op jit(solution)/shard_map/psum | solution.py:108
  670.5 0.7 slice.34
  671.2 117.9 %reduce-scatter.4.cloned.1.call-done = bf16[64,2048]{1,0:T(8,128)(2,1)} async-done(((bf16[2048,2048]{1,0:T(8,128)(2,1)}), bf16[64,2048]{1,0:T(8,128)(2,1)}) %reduce-scatter.4.cloned.1.call-update) | async-done | bytes 262160
  789.1 1.2 copy.43
  790.4 0.9 copy.37
  791.3 12.7 %all-to-all-start.4 = ((bf16[16,64,128]{2,1,0:T(8,128)(2,1)}), bf16[16,64,128]{2,1,0:T(8,128)(2,1)S(1)}, u32[]{:S(2)}, u32[]{:S(2)}) async-start(bf16[16,64,128]{2,1,0:T(8,128)(2,1)} %bitcast.29), calls=%async_computation.4 | async-start | bytes 524288 | tf_op jit(solution)/shard_map/all_to_all | solution.py:72
  803.9 0.5 fusion.84
  804.5 1.3 slice_multiply_fusion.5
  805.7 1.9 slice_multiply_fusion
  807.6 1.5 fusion.30
  809.1 12.2 %all-to-all-done.4 = bf16[16,64,128]{2,1,0:T(8,128)(2,1)S(1)} async-done(((bf16[16,64,128]{2,1,0:T(8,128)(2,1)}), bf16[16,64,128]{2,1,0:T(8,128)(2,1)S(1)}, u32[]{:S(2)}, u32[]{:S(2)}) %all-to-all-start.4) | async-done | bytes 262176 | tf_op jit(solution)/shard_map/all_to_all | solution.py:72
  821.3 0.1 copy.46
  821.4 0.7 copy.39
  (28 shorter events, 0.2 us)
Async XLA Ops:
  7.2 103.5 %copy-start = (bf16[1,128,2048]{2,1,0:T(8,128)(2,1)S(1)}, bf16[1,128,2048]{2,1,0:T(8,128)(2,1)}, u32[]{:S(2)}) copy-start(bf16[1,128,2048]{2,1,0:T(8,128)(2,1)} %param.8) | copy-start | bytes 1572868
  7.2 103.4 %all-gather.2.cloned.1.call-start = ((), (), s32[]{:S(2)}) async-start(), calls=%async_computation.6 | async-start | bytes 8650752 | tf_op jit(solution)/shard_map/all_gather | solution.py:37
  47.2 69.0 %all-to-all-start.1 = ((f32[16,2,2048]{2,1,0:T(2,128)}), f32[16,2,2048]{2,1,0:T(2,128)S(1)}, u32[]{:S(2)}, u32[]{:S(2)}) async-start(f32[16,2,2048]{2,1,0:T(2,128)} %broadcast_in_dim.11), calls=%async_computation.1 | async-start | bytes 524288 | tf_op jit(solution)/shard_map/all_to_all | solution.py:17
  56.1 72.8 %copy-start.5 = (bf16[128]{0:T(256)(128)(2,1)S(1)}, bf16[128]{0:T(256)(128)(2,1)}, u32[]{:S(2)}) copy-start(bf16[128]{0:T(256)(128)(2,1)} %param.14) | copy-start | bytes 772
  56.1 102.5 %copy-start.2 = (bf16[1,2048,128]{2,1,0:T(8,128)(2,1)S(1)}, bf16[1,2048,128]{2,1,0:T(8,128)(2,1)}, u32[]{:S(2)}) copy-start(bf16[1,2048,128]{2,1,0:T(8,128)(2,1)} %param.9) | copy-start | bytes 1572868
  56.1 104.0 %copy-start.1 = (bf16[1,2048,128]{2,1,0:T(8,128)(2,1)S(1)}, bf16[1,2048,128]{2,1,0:T(8,128)(2,1)}, u32[]{:S(2)}) copy-start(bf16[1,2048,128]{2,1,0:T(8,128)(2,1)} %param.10) | copy-start | bytes 1572868
  115.3 55.1 %copy-start.6 = (bf16[128]{0:T(256)(128)(2,1)S(1)}, bf16[128]{0:T(256)(128)(2,1)}, u32[]{:S(2)}) copy-start(bf16[128]{0:T(256)(128)(2,1)} %param.15) | copy-start | bytes 772
  116.2 42.4 %all-to-all-start = ((bf16[128,16,128]{2,0,1:T(8,128)(2,1)}), bf16[128,16,128]{2,0,1:T(8,128)(2,1)S(1)}, u32[]{:S(2)}, u32[]{:S(2)}) async-start(bf16[128,16,128]{2,0,1:T(8,128)(2,1)} %bitcast.135), calls=%async_computation | async-start | bytes 1048576 | tf_op jit(solution)/shard_map/all_to_all | solution.py:61
  159.1 1.0 copy-start.3
  164.2 24.4 %all-to-all-start.2 = ((f32[16,2,2048]{2,1,0:T(2,128)}), f32[16,2,2048]{2,1,0:T(2,128)S(1)}, u32[]{:S(2)}, u32[]{:S(2)}) async-start(f32[16,2,2048]{2,1,0:T(2,128)} %broadcast_in_dim.15), calls=%async_computation.2 | async-start | bytes 524288 | tf_op jit(solution)/shard_map/all_to_all | solution.py:17
  194.4 34.5 %all-to-all-start.3 = ((bf16[16,128,128]{2,1,0:T(8,128)(2,1)}), bf16[16,128,128]{2,1,0:T(8,128)(2,1)S(1)}, u32[]{:S(2)}, u32[]{:S(2)}) async-start(bf16[16,128,128]{2,1,0:T(8,128)(2,1)} %get-tuple-element.36), calls=%async_computation.3 | async-start | bytes 1048576 | tf_op jit(solution)/shard_map/all_to_all | solution.py:59
  200.5 470.0 %all-reduce.2.cloned.1.call-start = ((), (), s32[]{:S(2)}) async-start(), calls=%async_computation.7 | async-start | bytes 1089536 | tf_op jit(solution)/shard_map/psum | solution.py:108
  204.6 584.5 %reduce-scatter.4.cloned.1.call-start = ((), (), s32[]{:S(2)}) async-start(), calls=%async_computation.8 | async-start | bytes 8650752
  247.1 560.5 %copy-start.4 = (f32[16,128,128]{2,1,0:T(8,128)S(1)}, f32[16,128,128]{2,1,0:T(8,128)}, u32[]{:S(2)}) copy-start(f32[16,128,128]{2,1,0:T(8,128)} %get-tuple-element.37) | copy-start | bytes 3145732
  791.3 30.0 %all-to-all-start.4 = ((bf16[16,64,128]{2,1,0:T(8,128)(2,1)}), bf16[16,64,128]{2,1,0:T(8,128)(2,1)S(1)}, u32[]{:S(2)}, u32[]{:S(2)}) async-start(bf16[16,64,128]{2,1,0:T(8,128)(2,1)} %bitcast.29), calls=%async_computation.4 | async-start | bytes 524288 | tf_op jit(solution)/shard_map/all_to_all | solution.py:72
Sparse Core Ops, SparseCore 0:
  44.7 65.8 all-gather.1
  206.8 463.6 all-reduce.1
  675.1 114.0 reduce-scatter.3
where the time goes:
time: 830 us; the launch traced here: 829 us
  waiting for transfers between devices  679 us (82%)
  starting transfers between devices  46.6 us (6%)
  blocking collectives  37.3 us (4%)
  local copies, waits for them, and re-layouts  19.8 us (2%)
  matrix products  18.9 us (2%)
  between operations  13.9 us (2%)
  other arithmetic  12.7 us (2%)
    psum x1, waiting for transfers between devices, local(): total = lax.psum(packed, ('sp', 'dp'))  423 us
    unnamed x4, waiting for transfers between devices  118 us
    all_gather x1, waiting for transfers between devices, local(): weight_whole = lax.all_gather(weight_rows, 'dp', axis=0, tiled=True)  54.5 us
    all_gather x1, blocking collectives, local(): weight_rows = lax.all_gather(out_weight, 'sp', axis=1, tiled=True)  37.3 us
    all_to_all x1, waiting for transfers between devices, local(): lax.all_to_all(head_rows.astype(jnp.bfloat16), 'sp', split_axis=1, concat...  29.5 us
    all_to_all x1, waiting for transfers between devices, local(): lax.all_to_all(gated, 'sp', split_axis=0, concat_axis=1, tiled=True)  24.2 us
    all_to_all x2, waiting for transfers between devices, sum_over(): return lax.all_to_all(copies, axis, 0, 0, tiled=True).sum(axis=0)  17.5 us
  transfers between devices with their start and end apart: 8, of which 7 were waited for; matrix products, arithmetic and copies ran while one was open for 4% of the time, Pallas kernels for 0%

commit v1 on v0

--- a/solution.py
+++ b/solution.py
@@ -1,3 +1,4 @@
+import functools
 import math
 import jax
 import jax.numpy as jnp
@@ -9,6 +10,14 @@
 BLK = 128
 epsilon = 1e-05
 tanh_coef = math.sqrt(2.0 / math.pi)
+
+
+def _review_yards(own_rows, lane_axis, dev_axis):
+    u_next = lax.psum(own_rows, axis_name=lane_axis)
+    return lax.psum(u_next, axis_name=dev_axis)
+
+
+fit_windows = functools.partial(_review_yards, lane_axis="sp", dev_axis="dp")
 
 
 def sum_over(x, axis):
@@ -105,7 +114,7 @@
             own_hot[:, None] * shift_term,
         ]
     )
-    total = lax.psum(packed, ("sp", "dp"))
+    total = fit_windows(packed)
     top = GROUPS * BLK
     weight_total = total[:top].reshape(GROUPS, BLK, BLK)
     bias_total = total[top : top + GROUPS]

time: 830 us -> 635 us (0.77)
  waiting for transfers between devices: 679 us -> 485 us
    psum x1 -> x2, waiting for transfers between devices: 423 us -> 251 us  [the longest x1 137 us: _review_yards(): u_next = lax.psum(own_rows, axis_name=lane_axis)]
    all_to_all x1, waiting for transfers between devices: 24.2 us -> 0.01 us  [local(): lax.all_to_all(gated, 'sp', split_axis=0, concat_axis=1, tiled=True)]
    unnamed x4 -> x5, waiting for transfers between devices: 118 us -> 119 us
  transfers between devices with their start and end apart: 8 -> 9, of which waited for: 7 -> 7; matrix products, arithmetic and copies ran while one was open for 4% -> 6% of each run, Pallas kernels for 0% -> 0%
where the time goes in v1:
time: 635 us; the launch traced here: 634 us
  waiting for transfers between devices  485 us (76%)
  starting transfers between devices  46.6 us (7%)
  blocking collectives  37.3 us (6%)
  local copies, waits for them, and re-layouts  19.8 us (3%)
  matrix products  18.9 us (3%)
  between operations  13.9 us (2%)
  other arithmetic  12.7 us (2%)
    psum x1, waiting for transfers between devices, _review_yards(): u_next = lax.psum(own_rows, axis_name=lane_axis)  137 us
    unnamed x5, waiting for transfers between devices  119 us
    psum x1, waiting for transfers between devices, _review_yards(): return lax.psum(u_next, axis_name=dev_axis)  115 us
    all_gather x1, waiting for transfers between devices, local(): weight_whole = lax.all_gather(weight_rows, 'dp', axis=0, tiled=True)  54.5 us
    all_gather x1, blocking collectives, local(): weight_rows = lax.all_gather(out_weight, 'sp', axis=1, tiled=True)  37.3 us
    all_to_all x1, waiting for transfers between devices, local(): lax.all_to_all(head_rows.astype(jnp.bfloat16), 'sp', split_axis=1, concat...  29.5 us
    all_to_all x2, waiting for transfers between devices, sum_over(): return lax.all_to_all(copies, axis, 0, 0, tiled=True).sum(axis=0)  17.5 us
    unnamed x18, local copies, waits for them, and re-layouts  15.4 us
  transfers between devices with their start and end apart: 9, of which 7 were waited for; matrix products, arithmetic and copies ran while one was open for 6% of the time, Pallas kernels for 0%

profile of v1, /device:TPU:32, one launch (start us, length us, event | category | flops | bytes accessed | tf_op | source)
XLA Modules:
  0.0 634.0 jit_solution(1135314620933611738)
XLA Ops:
  7.2 0.0 all-gather.2.cloned.1.call-start
  7.2 37.3 %all_gather.6 = bf16[64,2048]{1,0:T(8,128)(2,1)} all-gather(bf16[64,128]{1,0:T(8,128)(2,1)} %param.11), channel_id=1, replica_groups=mesh['sp'=16,'dp'=32] {'sp'}, dimensions={1}, use_global_device_ids=true | all-gather | bytes 278528 | tf_op jit(solution)/shard_map/all_gather | solution.py:45
  44.6 1.8 fusion.58
  46.4 0.8 broadcast_in_dim.11
  47.2 8.9 %all-to-all-start.1 = ((f32[16,2,2048]{2,1,0:T(2,128)}), f32[16,2,2048]{2,1,0:T(2,128)S(1)}, u32[]{:S(2)}, u32[]{:S(2)}) async-start(f32[16,2,2048]{2,1,0:T(2,128)} %broadcast_in_dim.11), calls=%async_computation.1 | async-start | bytes 524288 | tf_op jit(solution)/shard_map/all_to_all | solution.py:26
  56.1 54.5 %all-gather.2.cloned.1.call-done = bf16[2048,2048]{1,0:T(8,128)(2,1)} async-done(((bf16[64,2048]{1,0:T(8,128)(2,1)}), bf16[2048,2048]{1,0:T(8,128)(2,1)}) %all-gather.2.cloned.1.call-update) | async-done | bytes 8388624 | tf_op jit(solution)/shard_map/all_gather | solution.py:46
  110.6 4.6 fusion.5
  115.3 0.9 copy.53
  116.2 12.7 %all-to-all-start = ((bf16[128,16,128]{2,0,1:T(8,128)(2,1)}), bf16[128,16,128]{2,0,1:T(8,128)(2,1)S(1)}, u32[]{:S(2)}, u32[]{:S(2)}) async-start(bf16[128,16,128]{2,0,1:T(8,128)(2,1)} %bitcast.135), calls=%async_computation | async-start | bytes 1048576 | tf_op jit(solution)/shard_map/all_to_all | solution.py:70
  128.9 0.1 reduce_sum.92
  129.0 29.5 %all-to-all-done = bf16[128,16,128]{2,0,1:T(8,128)(2,1)S(1)} async-done(((bf16[128,16,128]{2,0,1:T(8,128)(2,1)}), bf16[128,16,128]{2,0,1:T(8,128)(2,1)S(1)}, u32[]{:S(2)}, u32[]{:S(2)}) %all-to-all-start) | async-done | bytes 524320 | tf_op jit(solution)/shard_map/all_to_all | solution.py:70
  158.6 0.5 fusion.59
  159.1 1.0 copy-done.3
  160.1 3.3 fusion.56
  163.4 0.8 broadcast_in_dim.15
  164.2 6.1 all-to-all-start.2
  170.3 0.7 fusion.80
  171.0 17.5 %all-to-all-done.2 = f32[16,2,2048]{2,1,0:T(2,128)S(1)} async-done(((f32[16,2,2048]{2,1,0:T(2,128)}), f32[16,2,2048]{2,1,0:T(2,128)S(1)}, u32[]{:S(2)}, u32[]{:S(2)}) %all-to-all-start.2) | async-done | bytes 262176 | tf_op jit(solution)/shard_map/all_to_all | solution.py:26
  188.6 0.1 reduce_sum.95
  188.7 2.8 fusion.51
  191.5 3.0 multiply_convert_fusion
  194.4 6.1 all-to-all-start.3
  200.5 0.0 all-reduce.3.cloned.1.call-start
  200.6 0.3 reduce_sum.99
  200.8 0.1 broadcast_bitcast_fusion
  200.9 2.5 fusion.6
  203.5 0.2 bitcast_multiply_fusion.5
  203.7 0.1 broadcast_multiply_fusion.2
  203.7 0.9 pad_maximum_fusion
  204.6 0.0 all-reduce.5.cloned.1.call-start
  204.7 136.8 %all-reduce.3.cloned.1.call-done = f32[1064,128]{1,0:T(8,128)} async-done(((f32[1064,128]{1,0:T(8,128)}), f32[1064,128]{1,0:T(8,128)}) %all-reduce.3.cloned.1.call-update) | async-done | bytes 544784 | tf_op jit(solution)/shard_map/psum | solution.py:16
  341.5 0.0 reduce-scatter.4.cloned.1.call-start
  341.5 0.3 copy.36
  341.8 5.5 convert_bitcast_fusion
  347.4 12.3 %copy.42 = bf16[2048,2048]{1,0:T(8,128)(2,1)} copy(bf16[2048,2048]{0,1:T(8,128)(2,1)} %convert_bitcast_fusion) | data formatting | bytes 16777216
  359.7 114.7 %all-reduce.5.cloned.1.call-done = f32[1064,128]{1,0:T(8,128)} async-done(((f32[1064,128]{1,0:T(8,128)}), f32[1064,128]{1,0:T(8,128)}) %all-reduce.5.cloned.1.call-update) | async-done | bytes 544784 | tf_op jit(solution)/shard_map/psum | solution.py:17
  474.4 0.7 slice.34
  475.1 119.4 %reduce-scatter.4.cloned.1.call-done = bf16[64,2048]{1,0:T(8,128)(2,1)} async-done(((bf16[2048,2048]{1,0:T(8,128)(2,1)}), bf16[64,2048]{1,0:T(8,128)(2,1)}) %reduce-scatter.4.cloned.1.call-update) | async-done | bytes 262160
  594.5 1.2 copy.43
  595.7 0.9 copy.37
  596.6 12.7 %all-to-all-start.4 = ((bf16[16,64,128]{2,1,0:T(8,128)(2,1)}), bf16[16,64,128]{2,1,0:T(8,128)(2,1)S(1)}, u32[]{:S(2)}, u32[]{:S(2)}) async-start(bf16[16,64,128]{2,1,0:T(8,128)(2,1)} %bitcast.29), calls=%async_computation.4 | async-start | bytes 524288 | tf_op jit(solution)/shard_map/all_to_all | solution.py:81
  609.3 0.5 fusion.84
  609.8 1.3 slice_multiply_fusion.5
  611.1 1.9 slice_multiply_fusion
  612.9 1.5 fusion.30
  614.4 12.1 %all-to-all-done.4 = bf16[16,64,128]{2,1,0:T(8,128)(2,1)S(1)} async-done(((bf16[16,64,128]{2,1,0:T(8,128)(2,1)}), bf16[16,64,128]{2,1,0:T(8,128)(2,1)S(1)}, u32[]{:S(2)}, u32[]{:S(2)}) %all-to-all-start.4) | async-done | bytes 262176 | tf_op jit(solution)/shard_map/all_to_all | solution.py:81
  626.6 0.1 copy.46
  626.7 0.7 copy.39
  (31 shorter events, 0.3 us)
Async XLA Ops:
  7.2 103.5 %copy-start = (bf16[1,128,2048]{2,1,0:T(8,128)(2,1)S(1)}, bf16[1,128,2048]{2,1,0:T(8,128)(2,1)}, u32[]{:S(2)}) copy-start(bf16[1,128,2048]{2,1,0:T(8,128)(2,1)} %param.8) | copy-start | bytes 1572868
  7.2 103.4 %all-gather.2.cloned.1.call-start = ((), (), s32[]{:S(2)}) async-start(), calls=%async_computation.6 | async-start | bytes 8650752 | tf_op jit(solution)/shard_map/all_gather | solution.py:46
  47.2 69.0 %all-to-all-start.1 = ((f32[16,2,2048]{2,1,0:T(2,128)}), f32[16,2,2048]{2,1,0:T(2,128)S(1)}, u32[]{:S(2)}, u32[]{:S(2)}) async-start(f32[16,2,2048]{2,1,0:T(2,128)} %broadcast_in_dim.11), calls=%async_computation.1 | async-start | bytes 524288 | tf_op jit(solution)/shard_map/all_to_all | solution.py:26
  56.1 72.8 %copy-start.5 = (bf16[128]{0:T(256)(128)(2,1)S(1)}, bf16[128]{0:T(256)(128)(2,1)}, u32[]{:S(2)}) copy-start(bf16[128]{0:T(256)(128)(2,1)} %param.14) | copy-start | bytes 772
  56.1 102.5 %copy-start.2 = (bf16[1,2048,128]{2,1,0:T(8,128)(2,1)S(1)}, bf16[1,2048,128]{2,1,0:T(8,128)(2,1)}, u32[]{:S(2)}) copy-start(bf16[1,2048,128]{2,1,0:T(8,128)(2,1)} %param.9) | copy-start | bytes 1572868
  56.1 104.0 %copy-start.1 = (bf16[1,2048,128]{2,1,0:T(8,128)(2,1)S(1)}, bf16[1,2048,128]{2,1,0:T(8,128)(2,1)}, u32[]{:S(2)}) copy-start(bf16[1,2048,128]{2,1,0:T(8,128)(2,1)} %param.10) | copy-start | bytes 1572868
  115.3 55.1 %copy-start.6 = (bf16[128]{0:T(256)(128)(2,1)S(1)}, bf16[128]{0:T(256)(128)(2,1)}, u32[]{:S(2)}) copy-start(bf16[128]{0:T(256)(128)(2,1)} %param.15) | copy-start | bytes 772
  116.2 42.4 %all-to-all-start = ((bf16[128,16,128]{2,0,1:T(8,128)(2,1)}), bf16[128,16,128]{2,0,1:T(8,128)(2,1)S(1)}, u32[]{:S(2)}, u32[]{:S(2)}) async-start(bf16[128,16,128]{2,0,1:T(8,128)(2,1)} %bitcast.135), calls=%async_computation | async-start | bytes 1048576 | tf_op jit(solution)/shard_map/all_to_all | solution.py:70
  159.1 1.0 copy-start.3
  164.2 24.4 %all-to-all-start.2 = ((f32[16,2,2048]{2,1,0:T(2,128)}), f32[16,2,2048]{2,1,0:T(2,128)S(1)}, u32[]{:S(2)}, u32[]{:S(2)}) async-start(f32[16,2,2048]{2,1,0:T(2,128)} %broadcast_in_dim.15), calls=%async_computation.2 | async-start | bytes 524288 | tf_op jit(solution)/shard_map/all_to_all | solution.py:26
  194.4 147.1 %all-to-all-start.3 = ((bf16[16,128,128]{2,1,0:T(8,128)(2,1)}), bf16[16,128,128]{2,1,0:T(8,128)(2,1)S(1)}, u32[]{:S(2)}, u32[]{:S(2)}) async-start(bf16[16,128,128]{2,1,0:T(8,128)(2,1)} %get-tuple-element.36), calls=%async_computation.3 | async-start | bytes 1048576 | tf_op jit(solution)/shard_map/all_to_all | solution.py:68
  200.5 141.0 %all-reduce.3.cloned.1.call-start = ((), (), s32[]{:S(2)}) async-start(), calls=%async_computation.7 | async-start | bytes 1089536 | tf_op jit(solution)/shard_map/psum | solution.py:16
  204.6 269.8 %all-reduce.5.cloned.1.call-start = ((), (), s32[]{:S(2)}) async-start(), calls=%async_computation.8 | async-start | bytes 1089536 | tf_op jit(solution)/shard_map/psum | solution.py:17
  341.5 253.0 %reduce-scatter.4.cloned.1.call-start = ((), (), s32[]{:S(2)}) async-start(), calls=%async_computation.9 | async-start | bytes 8650752
  359.7 253.2 %copy-start.4 = (f32[16,128,128]{2,1,0:T(8,128)S(1)}, f32[16,128,128]{2,1,0:T(8,128)}, u32[]{:S(2)}) copy-start(f32[16,128,128]{2,1,0:T(8,128)} %get-tuple-element.37) | copy-start | bytes 3145732
  596.6 30.0 %all-to-all-start.4 = ((bf16[16,64,128]{2,1,0:T(8,128)(2,1)}), bf16[16,64,128]{2,1,0:T(8,128)(2,1)S(1)}, u32[]{:S(2)}, u32[]{:S(2)}) async-start(bf16[16,64,128]{2,1,0:T(8,128)(2,1)} %bitcast.29), calls=%async_computation.4 | async-start | bytes 524288 | tf_op jit(solution)/shard_map/all_to_all | solution.py:81
Sparse Core Ops, SparseCore 0:
  44.7 65.8 all-gather.1
  204.7 136.6 all-reduce.2
  344.7 129.6 all-reduce.4
  478.8 115.5 reduce-scatter.3
